TPU v7x, 32 devices: a whole 2x2x4 slice. The times are simulated.
32 devices in a mesh: gr: 2 (over x), fs: 8 (over z, y), tp: 2 (over core).
Axes of the slice: x: 2, y: 2, z: 4, core: 2. Of those that a mesh axis runs over, the one named last changes fastest.
Arguments:
- prompt_tokens: bfloat16 [4608, 2048], P(('gr', 'fs', 'tp')), may hold values from -6 to 6
- up_master: float32 [2048, 8192], P(('gr', 'fs'), 'tp'), may hold values from -0.125 to 0.125
- down_master: float32 [2048, 8192], P(('gr', 'fs'), 'tp'), may hold values from -0.0625 to 0.0625
- norm_gain: float32 [2048], P(('gr', 'fs')), may hold values from 0.1 to 1.9
Outputs:
- sampler_up: bfloat16 [2048, 8192], P(None, ('gr', 'tp'))
- sampler_down: bfloat16 [2048, 8192], P(None, ('gr', 'tp'))
- prompt_out: bfloat16 [4608, 2048], P(('gr', 'fs', 'tp'))
All inputs are finite; a program needn't handle non-finite values.
Results may differ from a plain program's by a relative error of at most 0.009.
Values may be sent and summed in bfloat16 or wider, within the bound.
A program may use at most 128 MiB of HBM per device.

v0:
```python
import functools

import jax
import jax.numpy as jnp
from jax import lax
from jax.experimental import pallas as pl
from jax.experimental.pallas import tpu as pltpu
from jax.sharding import PartitionSpec as P

MESH = pl.DeviceIdType.MESH
CHUNK = 32
TILE = 256
SPLIT = 4


def kernel(G, F, T, tok_in, gain_in, up_in, down_in, up_full, down_full, part,
           wide, narrow, raw, nrm, hid, stage,
           recv, sendl, sendr, sendy, send0, tok_recv, tok_send,
           part_recv, part_send, local_sem, load_sem):
    gr, f, tp = lax.axis_index("gr"), lax.axis_index("fs"), lax.axis_index("tp")
    full = (up_full, down_full)
    A = F // 2
    a, y = f // 2, f % 2
    mate = a * 2 + 1 - y
    R = up_in.shape[0]
    D, W = up_full.shape
    tok = tok_in.shape[0]
    CH = min(CHUNK, R)
    C = R // CH
    NQ = G * C
    PAIR_FIRST = (NQ * 5 // 32, (NQ * 5 + 31) // 32)
    K = G * T
    k = gr * T + tp
    weights = (up_in, down_in)

    def at_k(kk):
        return (kk // T, f, kk % T)

    def load(m, c):
        rows = pl.ds(c * CH, CH)
        return pltpu.make_async_copy(weights[m].at[rows], wide.at[m, rows], load_sem.at[m, c])

    token_load = pltpu.make_async_copy(tok_in, raw, local_sem.at[0])
    for c in range(C):
        load(0, c).start()
    token_load.start()
    for c in range(C):
        load(1, c).start()

    barrier = pltpu.get_barrier_semaphore()
    for d in range(1, K):
        pl.semaphore_signal(barrier, inc=1, device_id=at_k((k + d) % K), device_id_type=MESH)
    pl.semaphore_signal(barrier, inc=1, device_id=(gr, mate, tp), device_id_type=MESH)

    for shift in (1, A - 1):
        near = lax.rem(a + shift, A) * 2 + y
        pl.semaphore_signal(barrier, inc=1, device_id=(gr, near, tp), device_id_type=MESH)
    pl.semaphore_wait(barrier, K + 2)

    def rows_of(origin, g, c):
        return pl.ds(pl.multiple_of(g * (F * R) + origin * R + c * CH, CH), CH)

    home = k // G == tp

    def cast(m, c):
        rows = pl.ds(c * CH, CH)
        load(m, c).wait()
        value = wide[m, rows, :]
        if m == 0:
            value = value * column[c * CH:(c + 1) * CH]
        value = value.astype(jnp.bfloat16)
        narrow[m, rows, :] = value
        for b in range(G):
            @pl.when(tp * G + b == k)
            def _():
                full[m][rows_of(f, gr, c), :] = value[:, b * W:(b + 1) * W]

    def hand(m, b, c, wait):
        kk = tp * G + b
        q = ((gr - kk // T + G) % G) * C + c

        @pl.when(kk != k)
        def _():
            copy = pltpu.make_async_remote_copy(
                src_ref=narrow.at[m, pl.ds(c * CH, CH), pl.ds(b * W, W)],
                dst_ref=full[m].at[rows_of(f, gr, c)],
                send_sem=send0.at[m, b, c], recv_sem=recv.at[m, f, q],
                device_id=at_k(kk), device_id_type=MESH)
            if wait:
                copy.wait_send()
            else:
                copy.start()

    mine = pl.ds(pl.multiple_of(k * tok, 16), tok)

    def tokens(wait):
        for d in range(1, K):
            copy = pltpu.make_async_remote_copy(
                src_ref=nrm.at[mine], dst_ref=nrm.at[mine],
                send_sem=tok_send.at[d - 1], recv_sem=tok_recv.at[d - 1],
                device_id=at_k((k + d) % K), device_id_type=MESH)
            if wait:
                copy.wait_send()
            else:
                copy.start()

    def normalize(i, carry):
        values = raw[pl.ds(pl.multiple_of(i * 16, 16), 16), :].astype(jnp.float32)
        center = jnp.mean(values, axis=-1, keepdims=True)
        moved = values - center
        spread = jnp.mean(jnp.square(moved), axis=-1, keepdims=True)
        nrm[pl.ds(pl.multiple_of(k * tok + i * 16, 16), 16), :] = (
            moved * lax.rsqrt(spread + 1e-05)).astype(jnp.bfloat16)
        return carry

    rowed = lax.broadcasted_iota(jnp.int32, (R, R), 0) == lax.broadcasted_iota(jnp.int32, (R, R), 1)
    column = jnp.sum(jnp.where(rowed, gain_in[...], 0.0), axis=1, keepdims=True)

    cast(0, 0)
    for c in range(C):
        if c + 1 < C:
            cast(0, c + 1)
        else:
            cast(1, 0)
        for b in range(G):
            hand(0, b, c, False)

    def chunk(m, origin, q):
        return full[m].at[rows_of(origin, (gr + q // C) % G, q % C)]

    def send(m, origin, q, sems, target, wait):
        ref = chunk(m, origin, q)
        copy = pltpu.make_async_remote_copy(
            src_ref=ref, dst_ref=ref, send_sem=sems.at[m, origin, q], recv_sem=recv.at[m, origin, q],
            device_id=(gr, target, tp), device_id_type=MESH)
        if wait:
            copy.wait_send()
        else:
            copy.start()

    def arrived(m, origin, q):
        ref = chunk(m, origin, q)
        pltpu.make_async_copy(ref, ref, recv.at[m, origin, q]).wait()

    def left(m, origin, q, wait):
        @pl.when(a > 0)
        def _():
            send(m, origin, q, sendl, f - 2, wait)

    def right(m, origin, q, wait):
        @pl.when(a < A - 1)
        def _():
            send(m, origin, q, sendr, f + 2, wait)

    def loop(low, high, step):
        def go(i, carry):
            step(i)
            return carry
        if high > low:
            lax.fori_loop(low, high, go, 0)

    def own(m, wait=False):
        def step(q):
            if not wait:
                @pl.when(jnp.logical_or(q >= C, jnp.logical_not(home)))
                def _():
                    arrived(m, f, q)
            left(m, f, q, wait)
            right(m, f, q, wait)
            send(m, f, q, sendy, mate, wait)
        if m == 0:
            loop(0, NQ, step)
        else:
            loop(0, PAIR_FIRST[m], step)
            loop(C, NQ, step)
            loop(PAIR_FIRST[m], C, step)

    def mated(m, wait=False):
        def step(q):
            if not wait:
                arrived(m, mate, q)
            left(m, mate, q, wait)
            right(m, mate, q, wait)
        loop(0, PAIR_FIRST[m], step)

    def line(m, s, wait=False, between=None, eager=None):
        below, above = a - 1 - s, a + 1 + s

        def pass_on(origin_a, side, q, onward, across):
            origin = origin_a * 2 + side
            if not wait:
                arrived(m, origin, q)
            onward(m, origin, q, wait)
            if across:
                send(m, origin, q, sendy, mate, wait)

        def both(side, across):
            def step(q):
                @pl.when(below >= 0)
                def _():
                    pass_on(below, side, q, right, across)

                @pl.when(above < A)
                def _():
                    pass_on(above, side, q, left, across)
            return step

        pf = PAIR_FIRST[m]
        loop(0, pf, both(y, False))
        if m == 0:
            loop(pf, NQ, both(y, True))
        else:
            loop(C, NQ, both(y, True))
            if between is not None:
                between()
            loop(pf, C, both(y, True))
        if eager is not None:
            eager()
        loop(0, pf, both(1 - y, False))

    def settle(m, origin_a, gi):
        low = jnp.maximum(PAIR_FIRST[m], gi * C)

        def go(q, carry):
            arrived(m, origin_a * 2 + 1 - y, q)
            return carry
        lax.fori_loop(low, (gi + 1) * C, go, 0)

    def settle_all(i):
        for gi in range(G):
            settle(0, i, gi)

    own(0)
    token_load.wait()
    lax.fori_loop(0, tok // 16, normalize, 0)
    for c in range(C):
        if c + 1 < C:
            cast(1, c + 1)
        for b in range(G):
            hand(1, b, c, False)
    tokens(False)
    mated(0)
    loop(0, A - 2, lambda s: line(0, s))
    own(1)
    line(0, A - 2)
    mated(1)
    line(1, 0)

    loop(0, A, settle_all)
    for d in range(1, K):
        there = nrm.at[pl.ds(pl.multiple_of(((k - d + K) % K) * tok, 16), tok)]
        pltpu.make_async_copy(there, there, tok_recv.at[d - 1]).wait()

    tile = min(TILE, W)

    def lift(j):
        columns = pl.ds(pl.multiple_of(j * tile, tile), tile)
        lifted = jnp.maximum(jnp.dot(nrm[...], up_full[:, columns], preferred_element_type=jnp.float32), 0.0)
        hid[:, columns] = (lifted * lifted).astype(jnp.bfloat16)
    loop(0, W // tile, lift)

    def part_copy(d, block):
        target = (k + d) % K
        return pltpu.make_async_remote_copy(
            src_ref=stage.at[block, pl.ds(pl.multiple_of(target * tok, 16), tok)],
            dst_ref=part.at[d - 1, block],
            send_sem=part_send.at[d - 1, block], recv_sem=part_recv.at[d - 1, block],
            device_id=at_k(target), device_id_type=MESH)

    def lower(origin_a, gi):
        settle(1, origin_a, gi)
        g = (gr + gi) % G
        block = origin_a * G + g
        rows = pl.ds(pl.multiple_of(g * (F * R) + origin_a * (2 * R), 2 * R), 2 * R)
        value = lax.dot_general(hid[...], down_full[rows, :], (((1,), (1,)), ((), ())),
                                preferred_element_type=jnp.float32)
        stage[block] = value.astype(jnp.bfloat16)
        part[K - 1, block] = stage[block, mine]
        for d in range(1, K):
            part_copy(d, block).start()

    def lower_ring(s, low=0, high=G):
        @pl.when(a - 1 - s >= 0)
        def _():
            loop(low, high, lambda i: lower(a - 1 - s, G - 1 - i))

        @pl.when(a + 1 + s < A)
        def _():
            loop(low, high, lambda i: lower(a + 1 + s, G - 1 - i))

    loop(0, G, lambda i: lower(a, G - 1 - i))
    loop(1, A - 2, lambda s: line(1, s, between=lambda: lower_ring(s - 1)))
    line(1, A - 2, between=lambda: lower_ring(A - 3), eager=lambda: lower_ring(A - 2, 0, G - 1))
    lower_ring(A - 2, G - 1, G)

    for d in range(1, K):
        def landed(block):
            there = part.at[d - 1, block]
            pltpu.make_async_copy(there, there, part_recv.at[d - 1, block]).wait()
        loop(0, A * G, landed)

    def drain(block):
        for d in range(1, K):
            part_copy(d, block).wait_send()
    loop(0, A * G, drain)
    tokens(True)
    for m in range(2):
        for c in range(C):
            for b in range(G):
                hand(m, b, c, True)
        own(m, True)
        mated(m, True)
        loop(0, A - 1, lambda s: line(m, s, True))


def finish(G, F, up_held, down_held, parts, up_out, down_out, out_ref, sems):
    def out(m, i):
        source, target = ((up_held, up_out), (down_held, down_out))[m]
        size = source.shape[0] // SPLIT
        rows = pl.ds(i * size, size)
        return pltpu.make_async_copy(source.at[rows], target.at[rows], sems.at[m, i])

    for m in range(2):
        for i in range(SPLIT):
            out(m, i).start()
    K, blocks, _, wide = parts.shape
    D = out_ref.shape[1]
    for block in range(blocks):
        total = parts[0, block].astype(jnp.float32)
        for i in range(1, K):
            total += parts[i, block].astype(jnp.float32)
        begin = (block % G) * (D // G) + (block // G) * wide
        out_ref[:, begin:begin + wide] = total.astype(jnp.bfloat16)
    for m in range(2):
        for i in range(SPLIT):
            out(m, i).wait()


def body(G, F, T, prompt_tokens, up_master, down_master, norm_gain):
    R, width = up_master.shape
    tok = prompt_tokens.shape[0]
    D, W = R * G * F, width // G
    A, K = F // 2, G * T
    C = R // min(CHUNK, R)
    NQ = G * C
    bf16 = jnp.bfloat16
    any_space = pl.BlockSpec(memory_space=pl.ANY)
    vmem_space = pl.BlockSpec(memory_space=pltpu.VMEM)
    dma = pltpu.SemaphoreType.DMA
    up_held, down_held, parts = pl.pallas_call(
        functools.partial(kernel, G, F, T),
        name="handoff",
        out_shape=(
            pltpu.MemorySpace.VMEM((D, W), bf16),
            pltpu.MemorySpace.VMEM((D, W), bf16),
            pltpu.MemorySpace.VMEM((K, A * G, tok, 2 * R), bf16),
        ),
        in_specs=[any_space, vmem_space, any_space, any_space],
        out_specs=(vmem_space,) * 3,
        scratch_shapes=[
            pltpu.VMEM((2, R, width), jnp.float32),
            pltpu.VMEM((2, R, width), bf16),
            pltpu.VMEM((tok, D), bf16),
            pltpu.VMEM((K * tok, D), bf16),
            pltpu.VMEM((K * tok, W), bf16),
            pltpu.VMEM((A * G, K * tok, 2 * R), bf16),
            dma((2, F, NQ)), dma((2, F, NQ)), dma((2, F, NQ)), dma((2, F, NQ)),
            dma((2, G, C)), dma((K - 1,)), dma((K - 1,)),
            dma((K - 1, A * G)), dma((K - 1, A * G)), dma((1,)), dma((2, C)),
        ],
        compiler_params=pltpu.CompilerParams(
            collective_id=0, has_side_effects=True, vmem_limit_bytes=41 * 1024 * 1024),
    )(prompt_tokens, norm_gain.reshape(1, R), up_master, down_master)
    return pl.pallas_call(
        functools.partial(finish, G, F),
        name="finish",
        out_shape=(
            jax.ShapeDtypeStruct((D, W), bf16),
            jax.ShapeDtypeStruct((D, W), bf16),
            jax.ShapeDtypeStruct((tok, D), bf16),
        ),
        in_specs=[vmem_space] * 3,
        out_specs=(any_space, any_space, vmem_space),
        scratch_shapes=[dma((2, SPLIT))],
        compiler_params=pltpu.CompilerParams(vmem_limit_bytes=16 * 1024 * 1024),
    )(up_held, down_held, parts)


def solution(mesh):
    placed = (
        P(("gr", "fs", "tp"), None),
        P(("gr", "fs"), "tp"),
        P(("gr", "fs"), "tp"),
        P(("gr", "fs")),
    )
    return jax.shard_map(
        functools.partial(body, mesh.shape["gr"], mesh.shape["fs"], mesh.shape["tp"]),
        mesh=mesh,
        in_specs=placed,
        out_specs=(P(None, ("gr", "tp")), P(None, ("gr", "tp")), P(("gr", "fs", "tp"), None)),
        check_vma=False,
    )
```

profile of v0, /device:TPU:0, one launch (start us, length us, event | category | flops | bytes accessed | tf_op | source)
XLA Modules:
  0.0 185.2 jit_solution(7361861711681150747)
XLA Ops:
  0.6 177.9 %handoff.1 = (bf16[2048,2048]{1,0:T(8,128)(2,1)S(1)}, bf16[2048,2048]{1,0:T(8,128)(2,1)S(1)}, bf16[4,8,144,256]{3,2,1,0:T(8,128)(2,1)S(1)}) custom-call(bf16[144,2048]{1,0:T(8,128)(2,1)} %tok_in.1, f32[1,128]{1,0:T(1,128)} %bitcast.1, f32[128,4096]{1,0:T(8,128)} %up_in.1, f32[128,4096]{1,0:T(8,128)} %down_in.1), custom_call_target="tpu_custom_call" | custom-call | tf_op jit(solution)/shard_map/handoff/pallas_call | solution.py:350
  178.5 6.7 %finish.1 = (bf16[2048,2048]{1,0:T(8,128)(2,1)}, bf16[2048,2048]{1,0:T(8,128)(2,1)}, bf16[144,2048]{1,0:T(8,128)(2,1)}) custom-call(bf16[2048,2048]{1,0:T(8,128)(2,1)S(1)} %get-tuple-element.6.up_held, bf16[2048,2048]{1,0:T(8,128)(2,1)S(1)} %get-tuple-element.7.down_held, bf16[4,8,144,256]{3,2,1,0:T(8,128)(2,1)S(1)} %get-tuple-element.8.parts), custom_call_target="tpu_custom_call" | custom-call | tf_op jit(solution)/shard_map/finish/pallas_call | solution.py:374
where the time goes:
time: 185 us
  Pallas kernels  185 us (100%)
    pallas_call x1, Pallas kernels, body(): pl.pallas_call(functools.partial(kernel, G, F, T), name='handoff', out_sh...  178 us
    pallas_call x1, Pallas kernels, body(): pl.pallas_call(functools.partial(finish, G, F), name='finish', out_shape=...  6.74 us

commit v1 on v0

v1 whole, which is shorter than its diff:
```python
import functools

import jax
import jax.numpy as jnp
from jax import lax
from jax.experimental import pallas as pl
from jax.experimental.pallas import tpu as pltpu
from jax.sharding import PartitionSpec as P

MESH = pl.DeviceIdType.MESH
CHUNK = 32
TILE = 256
SPLIT = 4


def pair_first(count):
    return (count * 5 // 32, (count * 5 + 31) // 32)


def kernel(G, F, T, tok_in, gain_in, up_in, down_in, up_full, down_full, part,
           wide, narrow, raw, nrm, hid, stage,
           recv, dup, cross, cross_down, sendl, sendr, sendy, send0, tok_recv, tok_send,
           part_recv, part_send, local_sem, load_sem):
    gr, f, tp = lax.axis_index("gr"), lax.axis_index("fs"), lax.axis_index("tp")
    full = (up_full, down_full)
    A = F // 2
    a, y = f // 2, f % 2
    mate = a * 2 + 1 - y
    R = up_in.shape[0]
    D, W = up_full.shape
    tok = tok_in.shape[0]
    CH = min(CHUNK, R)
    C = R // CH
    NQ = G * C
    PAIR_FIRST = pair_first(NQ)
    K = G * T
    k = gr * T + tp
    weights = (up_in, down_in)

    def at_k(kk):
        return (kk // T, f, kk % T)

    def load(m, c):
        rows = pl.ds(c * CH, CH)
        return pltpu.make_async_copy(weights[m].at[rows], wide.at[m, rows], load_sem.at[m, c])

    barrier = pltpu.get_barrier_semaphore()

    @pl.when(a > 0)
    def _():
        pl.semaphore_signal(barrier, inc=1, device_id=(gr, f - 2, tp), device_id_type=MESH)

    @pl.when(a < A - 1)
    def _():
        pl.semaphore_signal(barrier, inc=1, device_id=(gr, f + 2, tp), device_id_type=MESH)
    pl.semaphore_signal(barrier, inc=1, device_id=(gr, mate, tp), device_id_type=MESH)
    for d in range(1, K):
        pl.semaphore_signal(barrier, inc=1, device_id=at_k((k + d) % K), device_id_type=MESH)

    token_load = pltpu.make_async_copy(tok_in, raw, local_sem.at[0])
    for c in range(C):
        load(0, c).start()
    for c in range(C):
        load(1, c).start()
    token_load.start()

    def rows_of(origin, g, c):
        return pl.ds(pl.multiple_of(g * (F * R) + origin * R + c * CH, CH), CH)

    home = k // G == tp

    def cast(m, c):
        rows = pl.ds(c * CH, CH)
        load(m, c).wait()
        value = wide[m, rows, :]
        if m == 0:
            value = value * column[c * CH:(c + 1) * CH]
        value = value.astype(jnp.bfloat16)
        narrow[m, rows, :] = value
        for b in range(G):
            @pl.when(tp * G + b == k)
            def _():
                full[m][rows_of(f, gr, c), :] = value[:, b * W:(b + 1) * W]

    def hand(m, b, c):
        kk = tp * G + b
        q = ((gr - kk // T + G) % G) * C + c

        @pl.when(kk != k)
        def _():
            copy = pltpu.make_async_remote_copy(
                src_ref=narrow.at[m, pl.ds(c * CH, CH), pl.ds(b * W, W)],
                dst_ref=full[m].at[rows_of(f, gr, c)],
                send_sem=send0.at[0], recv_sem=recv.at[m, a, q],
                device_id=at_k(kk), device_id_type=MESH)
            copy.start()

    mine = pl.ds(pl.multiple_of(k * tok, 16), tok)

    def tokens():
        for d in range(1, K):
            pltpu.make_async_remote_copy(
                src_ref=nrm.at[mine], dst_ref=nrm.at[mine],
                send_sem=tok_send.at[0], recv_sem=tok_recv.at[0],
                device_id=at_k((k + d) % K), device_id_type=MESH).start()

    def normalize(i, carry):
        values = raw[pl.ds(pl.multiple_of(i * 16, 16), 16), :].astype(jnp.float32)
        center = jnp.mean(values, axis=-1, keepdims=True)
        moved = values - center
        spread = jnp.mean(jnp.square(moved), axis=-1, keepdims=True)
        nrm[pl.ds(pl.multiple_of(k * tok + i * 16, 16), 16), :] = (
            moved * lax.rsqrt(spread + 1e-05)).astype(jnp.bfloat16)
        return carry

    rowed = lax.broadcasted_iota(jnp.int32, (R, R), 0) == lax.broadcasted_iota(jnp.int32, (R, R), 1)
    column = jnp.sum(jnp.where(rowed, gain_in[...], 0.0), axis=1, keepdims=True)

    for c in range(C):
        cast(0, c)
    pl.semaphore_wait(barrier, K + (a > 0).astype(jnp.int32) + (a < A - 1).astype(jnp.int32))
    for c in range(C):
        for b in range(G):
            hand(0, b, c)

    def chunk(m, origin, q):
        return full[m].at[rows_of(origin, (gr + q // C) % G, q % C)]

    def landing(m, origin_a, side, q):
        if side == "line":
            return recv.at[m, origin_a, q]
        if side == "pair":
            return dup.at[m, origin_a, q]
        return cross.at[0] if m == 0 else cross_down.at[origin_a, q // C]

    def send(m, origin, q, sem, side, target):
        ref = chunk(m, origin, q)
        pltpu.make_async_remote_copy(
            src_ref=ref, dst_ref=ref, send_sem=sem.at[0], recv_sem=landing(m, origin // 2, side, q),
            device_id=(gr, target, tp), device_id_type=MESH).start()

    def await_rows(ref, count, sem):
        if count > 0:
            rows = ref.at[pl.ds(0, count)]
            pltpu.make_async_copy(rows, rows, sem).wait()

    def arrived(m, origin, q, side="line"):
        ref = chunk(m, origin, q)
        pltpu.make_async_copy(ref, ref, landing(m, origin // 2, side, q)).wait()

    def left(m, origin, q, side="line"):
        @pl.when(a > 0)
        def _():
            send(m, origin, q, sendl, side, f - 2)

    def right(m, origin, q, side="line"):
        @pl.when(a < A - 1)
        def _():
            send(m, origin, q, sendr, side, f + 2)

    def loop(low, high, step):
        def go(i, carry):
            step(i)
            return carry
        if high > low:
            lax.fori_loop(low, high, go, 0)

    def own(m):
        def go(side):
            def step(q):
                @pl.when(jnp.logical_or(q >= C, jnp.logical_not(home)))
                def _():
                    arrived(m, f, q)
                left(m, f, q)
                right(m, f, q)
                send(m, f, q, sendy, side, mate)
            return step
        pf = PAIR_FIRST[m]
        loop(0, pf, go("pair"))
        if m == 0:
            loop(pf, NQ, go("cross"))
        else:
            loop(C, NQ, go("cross"))
            loop(pf, C, go("cross"))

    def mated(m):
        def step(q):
            arrived(m, mate, q, "pair")
            left(m, mate, q, "pair")
            right(m, mate, q, "pair")
        loop(0, PAIR_FIRST[m], step)

    def line(m, s, between=None, eager=None):
        below, above = a - 1 - s, a + 1 + s

        def pass_on(origin, side, q, onward, across):
            arrived(m, origin, q, side)
            onward(m, origin, q, side)
            if across:
                send(m, origin, q, sendy, "cross", mate)

        def both(side, across):
            def step(q):
                mine_y = y if side == "line" else 1 - y

                @pl.when(below >= 0)
                def _():
                    pass_on(below * 2 + mine_y, side, q, right, across)

                @pl.when(above < A)
                def _():
                    pass_on(above * 2 + mine_y, side, q, left, across)
            return step

        pf = PAIR_FIRST[m]
        loop(0, pf, both("line", False))
        if m == 0:
            loop(pf, NQ, both("line", True))
        else:
            loop(C, NQ, both("line", True))
            if between is not None:
                between()
            loop(pf, C, both("line", True))
        if eager is not None:
            eager()
        loop(0, pf, both("pair", False))

    def settle_down(origin_a, gi):
        if C > PAIR_FIRST[1]:
            @pl.when(gi == 0)
            def _():
                await_rows(down_full, (C - PAIR_FIRST[1]) * CH, cross_down.at[origin_a, 0])

        @pl.when(gi > 0)
        def _():
            await_rows(down_full, C * CH, cross_down.at[origin_a, gi])

    own(0)
    token_load.wait()
    lax.fori_loop(0, tok // 16, normalize, 0)
    for c in range(C):
        cast(1, c)
        for b in range(G):
            hand(1, b, c)
    tokens()
    mated(0)
    loop(0, A - 2, lambda s: line(0, s))
    own(1)
    line(0, A - 2)
    mated(1)
    line(1, 0)

    await_rows(up_full, A * (NQ - PAIR_FIRST[0]) * CH, cross.at[0])
    await_rows(nrm, (K - 1) * tok, tok_recv.at[0])

    tile = min(TILE, W)

    def lift(j):
        columns = pl.ds(pl.multiple_of(j * tile, tile), tile)
        lifted = jnp.maximum(jnp.dot(nrm[...], up_full[:, columns], preferred_element_type=jnp.float32), 0.0)
        hid[:, columns] = (lifted * lifted).astype(jnp.bfloat16)
    loop(0, W // tile, lift)

    def part_copy(d, block):
        target = (k + d) % K
        return pltpu.make_async_remote_copy(
            src_ref=stage.at[block, pl.ds(pl.multiple_of(target * tok, 16), tok)],
            dst_ref=part.at[d - 1, block],
            send_sem=part_send.at[0], recv_sem=part_recv.at[0],
            device_id=at_k(target), device_id_type=MESH)

    def lower(origin_a, gi):
        settle_down(origin_a, gi)
        g = (gr + gi) % G
        block = origin_a * G + g
        rows = pl.ds(pl.multiple_of(g * (F * R) + origin_a * (2 * R), 2 * R), 2 * R)
        value = lax.dot_general(hid[...], down_full[rows, :], (((1,), (1,)), ((), ())),
                                preferred_element_type=jnp.float32)
        stage[block] = value.astype(jnp.bfloat16)
        part[K - 1, block] = stage[block, mine]
        for d in range(1, K):
            part_copy(d, block).start()

    def lower_ring(s, low=0, high=G):
        @pl.when(a - 1 - s >= 0)
        def _():
            loop(low, high, lambda i: lower(a - 1 - s, G - 1 - i))

        @pl.when(a + 1 + s < A)
        def _():
            loop(low, high, lambda i: lower(a + 1 + s, G - 1 - i))

    loop(0, G, lambda i: lower(a, G - 1 - i))
    loop(1, A - 2, lambda s: line(1, s, between=lambda: lower_ring(s - 1)))
    line(1, A - 2, between=lambda: lower_ring(A - 3), eager=lambda: lower_ring(A - 2, 0, G - 1))
    lower_ring(A - 2, G - 1, G)

    await_rows(part, K - 1, part_recv.at[0])
    await_rows(part, K - 1, part_send.at[0])
    await_rows(nrm, (K - 1) * tok, tok_send.at[0])
    pairs = sum(PAIR_FIRST)
    await_rows(up_full, 2 * NQ * CH, sendy.at[0])
    for _ in range(A - 1):
        await_rows(up_full, (2 * NQ - pairs) * CH, sendy.at[0])

    def drain(sem, rows):
        def step(i, carry):
            await_rows(up_full, rows, sem.at[0])
            return carry
        return step
    lax.fori_loop(0, jnp.where(a > 0, A - a, 0), drain(sendl, (2 * NQ + pairs) * CH), 0)
    lax.fori_loop(0, jnp.where(a < A - 1, a + 1, 0), drain(sendr, (2 * NQ + pairs) * CH), 0)
    lax.fori_loop(0, jnp.where(home, G - 1, G), drain(send0, 2 * R), 0)


def finish(G, F, up_held, down_held, parts, up_out, down_out, out_ref, sems):
    def out(m, i):
        source, target = ((up_held, up_out), (down_held, down_out))[m]
        size = source.shape[0] // SPLIT
        rows = pl.ds(i * size, size)
        return pltpu.make_async_copy(source.at[rows], target.at[rows], sems.at[m, i])

    for m in range(2):
        for i in range(SPLIT):
            out(m, i).start()
    K, blocks, _, wide = parts.shape
    D = out_ref.shape[1]
    for block in range(blocks):
        total = parts[0, block].astype(jnp.float32)
        for i in range(1, K):
            total += parts[i, block].astype(jnp.float32)
        begin = (block % G) * (D // G) + (block // G) * wide
        out_ref[:, begin:begin + wide] = total.astype(jnp.bfloat16)
    for m in range(2):
        for i in range(SPLIT):
            out(m, i).wait()


def body(G, F, T, prompt_tokens, up_master, down_master, norm_gain):
    R, width = up_master.shape
    tok = prompt_tokens.shape[0]
    D, W = R * G * F, width // G
    A, K = F // 2, G * T
    C = R // min(CHUNK, R)
    NQ = G * C
    bf16 = jnp.bfloat16
    any_space = pl.BlockSpec(memory_space=pl.ANY)
    vmem_space = pl.BlockSpec(memory_space=pltpu.VMEM)
    dma = pltpu.SemaphoreType.DMA
    up_held, down_held, parts = pl.pallas_call(
        functools.partial(kernel, G, F, T),
        name="handoff",
        out_shape=(
            pltpu.MemorySpace.VMEM((D, W), bf16),
            pltpu.MemorySpace.VMEM((D, W), bf16),
            pltpu.MemorySpace.VMEM((K, A * G, tok, 2 * R), bf16),
        ),
        in_specs=[any_space, vmem_space, any_space, any_space],
        out_specs=(vmem_space,) * 3,
        scratch_shapes=[
            pltpu.VMEM((2, R, width), jnp.float32),
            pltpu.VMEM((2, R, width), bf16),
            pltpu.VMEM((tok, D), bf16),
            pltpu.VMEM((K * tok, D), bf16),
            pltpu.VMEM((K * tok, W), bf16),
            pltpu.VMEM((A * G, K * tok, 2 * R), bf16),
            dma((2, A, NQ)), dma((2, A, max(1, max(pair_first(NQ))))), dma((1,)), dma((A, G)),
            dma((1,)), dma((1,)), dma((1,)), dma((1,)), dma((1,)), dma((1,)),
            dma((1,)), dma((1,)), dma((1,)), dma((2, C)),
        ],
        compiler_params=pltpu.CompilerParams(
            collective_id=0, has_side_effects=True, vmem_limit_bytes=41 * 1024 * 1024),
    )(prompt_tokens, norm_gain.reshape(1, R), up_master, down_master)
    return pl.pallas_call(
        functools.partial(finish, G, F),
        name="finish",
        out_shape=(
            jax.ShapeDtypeStruct((D, W), bf16),
            jax.ShapeDtypeStruct((D, W), bf16),
            jax.ShapeDtypeStruct((tok, D), bf16),
        ),
        in_specs=[vmem_space] * 3,
        out_specs=(any_space, any_space, vmem_space),
        scratch_shapes=[dma((2, SPLIT))],
        compiler_params=pltpu.CompilerParams(vmem_limit_bytes=16 * 1024 * 1024),
    )(up_held, down_held, parts)


def solution(mesh):
    placed = (
        P(("gr", "fs", "tp"), None),
        P(("gr", "fs"), "tp"),
        P(("gr", "fs"), "tp"),
        P(("gr", "fs")),
    )
    return jax.shard_map(
        functools.partial(body, mesh.shape["gr"], mesh.shape["fs"], mesh.shape["tp"]),
        mesh=mesh,
        in_specs=placed,
        out_specs=(P(None, ("gr", "tp")), P(None, ("gr", "tp")), P(("gr", "fs", "tp"), None)),
        check_vma=False,
    )
```

time: 185 us -> 180 us (0.973)
  Pallas kernels: 185 us -> 179 us
    pallas_call x1, Pallas kernels: 178 us -> 172 us  [body(): pl.pallas_call(functools.partial(kernel, G, F, T), name='handoff', out_sh...]
where the time goes in v1:
time: 180 us
  Pallas kernels  179 us (99%)
    pallas_call x1, Pallas kernels, body(): pl.pallas_call(functools.partial(kernel, G, F, T), name='handoff', out_sh...  172 us
    pallas_call x1, Pallas kernels, body(): pl.pallas_call(functools.partial(finish, G, F), name='finish', out_shape=...  6.74 us

profile of v1, /device:TPU:0, one launch (start us, length us, event | category | flops | bytes accessed | tf_op | source)
XLA Modules:
  0.0 179.6 jit_solution(9316651795601604270)
XLA Ops:
  0.6 172.2 %handoff.1 = (bf16[2048,2048]{1,0:T(8,128)(2,1)S(1)}, bf16[2048,2048]{1,0:T(8,128)(2,1)S(1)}, bf16[4,8,144,256]{3,2,1,0:T(8,128)(2,1)S(1)}) custom-call(bf16[144,2048]{1,0:T(8,128)(2,1)} %tok_in.1, f32[1,128]{1,0:T(1,128)} %bitcast.1, f32[128,4096]{1,0:T(8,128)} %up_in.1, f32[128,4096]{1,0:T(8,128)} %down_in.1), custom_call_target="tpu_custom_call" | custom-call | tf_op jit(solution)/shard_map/handoff/pallas_call | solution.py:350
  172.8 6.7 %finish.1 = (bf16[2048,2048]{1,0:T(8,128)(2,1)}, bf16[2048,2048]{1,0:T(8,128)(2,1)}, bf16[144,2048]{1,0:T(8,128)(2,1)}) custom-call(bf16[2048,2048]{1,0:T(8,128)(2,1)S(1)} %get-tuple-element.6.up_held, bf16[2048,2048]{1,0:T(8,128)(2,1)S(1)} %get-tuple-element.7.down_held, bf16[4,8,144,256]{3,2,1,0:T(8,128)(2,1)S(1)} %get-tuple-element.8.parts), custom_call_target="tpu_custom_call" | custom-call | tf_op jit(solution)/shard_map/finish/pallas_call | solution.py:374

commit v2 on v1

--- a/solution.py
+++ b/solution.py
@@ -13,8 +13,11 @@
 SPLIT = 4
 
 
-def pair_first(count):
-    return (count * 5 // 32, (count * 5 + 31) // 32)
+def pair_share(count, width):
+    share = []
+    for quarters in (count * 5 // 8, count * 6 // 8):
+        share.append((quarters // 4, quarters % 4 * (width // 4)))
+    return share
 
 
 def kernel(G, F, T, tok_in, gain_in, up_in, down_in, up_full, down_full, part,
@@ -32,7 +35,7 @@
     CH = min(CHUNK, R)
     C = R // CH
     NQ = G * C
-    PAIR_FIRST = pair_first(NQ)
+    share = pair_share(NQ, W)
     K = G * T
     k = gr * T + tp
     weights = (up_in, down_in)
@@ -43,6 +46,9 @@
     def load(m, c):
         rows = pl.ds(c * CH, CH)
         return pltpu.make_async_copy(weights[m].at[rows], wide.at[m, rows], load_sem.at[m, c])
+
+    for c in range(C):
+        load(0, c).start()
 
     barrier = pltpu.get_barrier_semaphore()
 
@@ -58,8 +64,6 @@
         pl.semaphore_signal(barrier, inc=1, device_id=at_k((k + d) % K), device_id_type=MESH)
 
     token_load = pltpu.make_async_copy(tok_in, raw, local_sem.at[0])
-    for c in range(C):
-        load(0, c).start()
     for c in range(C):
         load(1, c).start()
     token_load.start()
@@ -116,15 +120,9 @@
     rowed = lax.broadcasted_iota(jnp.int32, (R, R), 0) == lax.broadcasted_iota(jnp.int32, (R, R), 1)
     column = jnp.sum(jnp.where(rowed, gain_in[...], 0.0), axis=1, keepdims=True)
 
-    for c in range(C):
-        cast(0, c)
-    pl.semaphore_wait(barrier, K + (a > 0).astype(jnp.int32) + (a < A - 1).astype(jnp.int32))
-    for c in range(C):
-        for b in range(G):
-            hand(0, b, c)
-
-    def chunk(m, origin, q):
-        return full[m].at[rows_of(origin, (gr + q // C) % G, q % C)]
+    def chunk(m, origin, q, columns):
+        rows = rows_of(origin, (gr + q // C) % G, q % C)
+        return full[m].at[rows, pl.ds(columns[0], columns[1] - columns[0])]
 
     def landing(m, origin_a, side, q):
         if side == "line":
@@ -133,8 +131,10 @@
             return dup.at[m, origin_a, q]
         return cross.at[0] if m == 0 else cross_down.at[origin_a, q // C]
 
-    def send(m, origin, q, sem, side, target):
-        ref = chunk(m, origin, q)
+    whole = (0, W)
+
+    def send(m, origin, q, sem, side, target, columns=whole):
+        ref = chunk(m, origin, q, columns)
         pltpu.make_async_remote_copy(
             src_ref=ref, dst_ref=ref, send_sem=sem.at[0], recv_sem=landing(m, origin // 2, side, q),
             device_id=(gr, target, tp), device_id_type=MESH).start()
@@ -144,19 +144,19 @@
             rows = ref.at[pl.ds(0, count)]
             pltpu.make_async_copy(rows, rows, sem).wait()
 
-    def arrived(m, origin, q, side="line"):
-        ref = chunk(m, origin, q)
+    def arrived(m, origin, q, side="line", columns=whole):
+        ref = chunk(m, origin, q, columns)
         pltpu.make_async_copy(ref, ref, landing(m, origin // 2, side, q)).wait()
 
-    def left(m, origin, q, side="line"):
+    def left(m, origin, q, side="line", columns=whole):
         @pl.when(a > 0)
         def _():
-            send(m, origin, q, sendl, side, f - 2)
-
-    def right(m, origin, q, side="line"):
+            send(m, origin, q, sendl, side, f - 2, columns)
+
+    def right(m, origin, q, side="line", columns=whole):
         @pl.when(a < A - 1)
         def _():
-            send(m, origin, q, sendr, side, f + 2)
+            send(m, origin, q, sendr, side, f + 2, columns)
 
     def loop(low, high, step):
         def go(i, carry):
@@ -165,75 +165,129 @@
         if high > low:
             lax.fori_loop(low, high, go, 0)
 
+    def over_line(m):
+        pf, shared = share[m]
+        first = pf + (shared > 0)
+        return ([(0, pf, ())] if pf else []) + ([(pf, first, (shared, W))] if shared else []), (first, C, whole)
+
+    def over_pair(m):
+        pf, shared = share[m]
+        return ([(0, pf, whole)] if pf else []) + ([(pf, pf + 1, (0, shared))] if shared else [])
+
+    def across(m, origin, q, columns):
+        if columns:
+            send(m, origin, q, sendy, "cross", mate, columns)
+
+    def own_chunk(m, q, columns):
+        left(m, f, q)
+        right(m, f, q)
+        if not columns:
+            send(m, f, q, sendy, "pair", mate)
+        elif columns[0] > 0:
+            send(m, f, q, sendy, "pair", mate, (0, columns[0]))
+        across(m, f, q, columns)
+
     def own(m):
-        def go(side):
+        def near(columns):
             def step(q):
-                @pl.when(jnp.logical_or(q >= C, jnp.logical_not(home)))
-                def _():
-                    arrived(m, f, q)
-                left(m, f, q)
-                right(m, f, q)
-                send(m, f, q, sendy, side, mate)
+                if m == 0:
+                    @pl.when(jnp.logical_not(home))
+                    def _():
+                        arrived(m, f, q)
+                        own_chunk(m, q, columns)
+                else:
+                    @pl.when(jnp.logical_not(home))
+                    def _():
+                        arrived(m, f, q)
+                    own_chunk(m, q, columns)
             return step
-        pf = PAIR_FIRST[m]
-        loop(0, pf, go("pair"))
+
+        def far(q):
+            arrived(m, f, q)
+            own_chunk(m, q, whole)
+
+        shared, rest = over_line(m)
+        for low, high, columns in shared:
+            loop(low, high, near(columns))
         if m == 0:
-            loop(pf, NQ, go("cross"))
+            loop(rest[0], rest[1], near(whole))
+            loop(C, NQ, far)
         else:
-            loop(C, NQ, go("cross"))
-            loop(pf, C, go("cross"))
+            loop(C, NQ, far)
+            loop(rest[0], rest[1], near(whole))
 
     def mated(m):
-        def step(q):
-            arrived(m, mate, q, "pair")
-            left(m, mate, q, "pair")
-            right(m, mate, q, "pair")
-        loop(0, PAIR_FIRST[m], step)
+        for low, high, columns in over_pair(m):
+            def step(q):
+                arrived(m, mate, q, "pair", columns)
+                left(m, mate, q, "pair", columns)
+                right(m, mate, q, "pair", columns)
+            loop(low, high, step)
 
     def line(m, s, between=None, eager=None):
         below, above = a - 1 - s, a + 1 + s
 
-        def pass_on(origin, side, q, onward, across):
-            arrived(m, origin, q, side)
-            onward(m, origin, q, side)
-            if across:
-                send(m, origin, q, sendy, "cross", mate)
-
-        def both(side, across):
+        def both(side, columns):
+            sent = columns if side == "pair" else whole
+
+            def pass_on(origin, q, onward):
+                arrived(m, origin, q, side, sent)
+                onward(m, origin, q, side, sent)
+                if side == "line":
+                    across(m, origin, q, columns)
+
             def step(q):
                 mine_y = y if side == "line" else 1 - y
 
                 @pl.when(below >= 0)
                 def _():
-                    pass_on(below * 2 + mine_y, side, q, right, across)
+                    pass_on(below * 2 + mine_y, q, right)
 
                 @pl.when(above < A)
                 def _():
-                    pass_on(above * 2 + mine_y, side, q, left, across)
+                    pass_on(above * 2 + mine_y, q, left)
             return step
 
-        pf = PAIR_FIRST[m]
-        loop(0, pf, both("line", False))
+        shared, rest = over_line(m)
+        for low, high, columns in shared:
+            loop(low, high, both("line", columns))
         if m == 0:
-            loop(pf, NQ, both("line", True))
+            loop(rest[0], rest[1], both("line", whole))
+            loop(C, NQ, both("line", whole))
         else:
-            loop(C, NQ, both("line", True))
+            loop(C, NQ, both("line", whole))
             if between is not None:
                 between()
-            loop(pf, C, both("line", True))
+            loop(rest[0], rest[1], both("line", whole))
         if eager is not None:
             eager()
-        loop(0, pf, both("pair", False))
+        for low, high, columns in over_pair(m):
+            loop(low, high, both("pair", columns))
+
+    def pair_rows(m):
+        pf, shared = share[m]
+        return pf * CH + CH * shared // W
 
     def settle_down(origin_a, gi):
-        if C > PAIR_FIRST[1]:
-            @pl.when(gi == 0)
-            def _():
-                await_rows(down_full, (C - PAIR_FIRST[1]) * CH, cross_down.at[origin_a, 0])
+        @pl.when(gi == 0)
+        def _():
+            await_rows(down_full, C * CH - pair_rows(1), cross_down.at[origin_a, 0])
 
         @pl.when(gi > 0)
         def _():
             await_rows(down_full, C * CH, cross_down.at[origin_a, gi])
+
+    for c in range(C):
+        cast(0, c)
+        if c == 0:
+            pl.semaphore_wait(barrier, K + (a > 0).astype(jnp.int32) + (a < A - 1).astype(jnp.int32))
+
+        @pl.when(home)
+        def _():
+            pf, shared = share[0]
+            own_chunk(0, c, () if c < pf else (shared if c == pf else 0, W))
+        for b in range(G):
+            hand(0, b, c)
 
     own(0)
     token_load.wait()
@@ -250,7 +304,7 @@
     mated(1)
     line(1, 0)
 
-    await_rows(up_full, A * (NQ - PAIR_FIRST[0]) * CH, cross.at[0])
+    await_rows(up_full, A * (NQ * CH - pair_rows(0)), cross.at[0])
     await_rows(nrm, (K - 1) * tok, tok_recv.at[0])
 
     tile = min(TILE, W)
@@ -261,25 +315,56 @@
         hid[:, columns] = (lifted * lifted).astype(jnp.bfloat16)
     loop(0, W // tile, lift)
 
-    def part_copy(d, block):
+    halves = 2 if R % 128 == 0 else 1
+
+    def part_copy(d, block, columns):
         target = (k + d) % K
         return pltpu.make_async_remote_copy(
-            src_ref=stage.at[block, pl.ds(pl.multiple_of(target * tok, 16), tok)],
-            dst_ref=part.at[d - 1, block],
+            src_ref=stage.at[block, pl.ds(pl.multiple_of(target * tok, 16), tok), columns],
+            dst_ref=part.at[d - 1, block, :, columns],
             send_sem=part_send.at[0], recv_sem=part_recv.at[0],
             device_id=at_k(target), device_id_type=MESH)
+
+    def multiply(block, rows, columns):
+        value = lax.dot_general(hid[...], down_full[rows, :], (((1,), (1,)), ((), ())),
+                                preferred_element_type=jnp.float32)
+        stage[block, :, columns] = value.astype(jnp.bfloat16)
+        part[K - 1, block, :, columns] = stage[block, mine, columns]
+        for d in range(1, K):
+            part_copy(d, block, columns).start()
 
     def lower(origin_a, gi):
         settle_down(origin_a, gi)
         g = (gr + gi) % G
-        block = origin_a * G + g
         rows = pl.ds(pl.multiple_of(g * (F * R) + origin_a * (2 * R), 2 * R), 2 * R)
-        value = lax.dot_general(hid[...], down_full[rows, :], (((1,), (1,)), ((), ())),
-                                preferred_element_type=jnp.float32)
-        stage[block] = value.astype(jnp.bfloat16)
-        part[K - 1, block] = stage[block, mine]
-        for d in range(1, K):
-            part_copy(d, block).start()
+        multiply(origin_a * G + g, rows, pl.ds(0, 2 * R))
+
+    def lower_half(origin_a, side):
+        rows = pl.ds(pl.multiple_of(gr * (F * R) + (origin_a * 2 + side) * R, R), R)
+        multiply(origin_a * G + gr, rows, pl.ds(pl.multiple_of(side * R, R), R))
+
+    def ends(step):
+        @pl.when(a - 1 - (A - 2) >= 0)
+        def _():
+            step(a - 1 - (A - 2))
+
+        @pl.when(a + 1 + (A - 2) < A)
+        def _():
+            step(a + 1 + (A - 2))
+
+    def early():
+        lower_ring(A - 2, 0, G - 1)
+        if halves == 2:
+            ends(lambda origin_a: lower_half(origin_a, y))
+
+    def late():
+        if halves == 2:
+            def step(origin_a):
+                settle_down(origin_a, 0)
+                lower_half(origin_a, 1 - y)
+            ends(step)
+        else:
+            lower_ring(A - 2, G - 1, G)
 
     def lower_ring(s, low=0, high=G):
         @pl.when(a - 1 - s >= 0)
@@ -292,28 +377,28 @@
 
     loop(0, G, lambda i: lower(a, G - 1 - i))
     loop(1, A - 2, lambda s: line(1, s, between=lambda: lower_ring(s - 1)))
-    line(1, A - 2, between=lambda: lower_ring(A - 3), eager=lambda: lower_ring(A - 2, 0, G - 1))
-    lower_ring(A - 2, G - 1, G)
+    line(1, A - 2, between=lambda: lower_ring(A - 3), eager=early)
+    late()
 
     await_rows(part, K - 1, part_recv.at[0])
     await_rows(part, K - 1, part_send.at[0])
     await_rows(nrm, (K - 1) * tok, tok_send.at[0])
-    pairs = sum(PAIR_FIRST)
+    pairs = pair_rows(0) + pair_rows(1)
     await_rows(up_full, 2 * NQ * CH, sendy.at[0])
     for _ in range(A - 1):
-        await_rows(up_full, (2 * NQ - pairs) * CH, sendy.at[0])
+        await_rows(up_full, 2 * NQ * CH - pairs, sendy.at[0])
 
     def drain(sem, rows):
         def step(i, carry):
             await_rows(up_full, rows, sem.at[0])
             return carry
         return step
-    lax.fori_loop(0, jnp.where(a > 0, A - a, 0), drain(sendl, (2 * NQ + pairs) * CH), 0)
-    lax.fori_loop(0, jnp.where(a < A - 1, a + 1, 0), drain(sendr, (2 * NQ + pairs) * CH), 0)
+    lax.fori_loop(0, jnp.where(a > 0, A - a, 0), drain(sendl, 2 * NQ * CH + pairs), 0)
+    lax.fori_loop(0, jnp.where(a < A - 1, a + 1, 0), drain(sendr, 2 * NQ * CH + pairs), 0)
     lax.fori_loop(0, jnp.where(home, G - 1, G), drain(send0, 2 * R), 0)
 
 
-def finish(G, F, up_held, down_held, parts, up_out, down_out, out_ref, sems):
+def finish(G, F, up_held, down_held, parts, up_out, down_out, out_ref, summed, sems, out_sem):
     def out(m, i):
         source, target = ((up_held, up_out), (down_held, down_out))[m]
         size = source.shape[0] // SPLIT
@@ -330,10 +415,13 @@
         for i in range(1, K):
             total += parts[i, block].astype(jnp.float32)
         begin = (block % G) * (D // G) + (block // G) * wide
-        out_ref[:, begin:begin + wide] = total.astype(jnp.bfloat16)
+        summed[:, begin:begin + wide] = total.astype(jnp.bfloat16)
+    tokens_out = pltpu.make_async_copy(summed, out_ref, out_sem.at[0])
+    tokens_out.start()
     for m in range(2):
         for i in range(SPLIT):
             out(m, i).wait()
+    tokens_out.wait()
 
 
 def body(G, F, T, prompt_tokens, up_master, down_master, norm_gain):
@@ -343,6 +431,7 @@
     A, K = F // 2, G * T
     C = R // min(CHUNK, R)
     NQ = G * C
+    pairs = max(1, max(pf + (shared > 0) for pf, shared in pair_share(NQ, W)))
     bf16 = jnp.bfloat16
     any_space = pl.BlockSpec(memory_space=pl.ANY)
     vmem_space = pl.BlockSpec(memory_space=pltpu.VMEM)
@@ -364,7 +453,7 @@
             pltpu.VMEM((K * tok, D), bf16),
             pltpu.VMEM((K * tok, W), bf16),
             pltpu.VMEM((A * G, K * tok, 2 * R), bf16),
-            dma((2, A, NQ)), dma((2, A, max(1, max(pair_first(NQ))))), dma((1,)), dma((A, G)),
+            dma((2, A, NQ)), dma((2, A, pairs)), dma((1,)), dma((A, G)),
             dma((1,)), dma((1,)), dma((1,)), dma((1,)), dma((1,)), dma((1,)),
             dma((1,)), dma((1,)), dma((1,)), dma((2, C)),
         ],
@@ -380,8 +469,8 @@
             jax.ShapeDtypeStruct((tok, D), bf16),
         ),
         in_specs=[vmem_space] * 3,
-        out_specs=(any_space, any_space, vmem_space),
-        scratch_shapes=[dma((2, SPLIT))],
+        out_specs=(any_space, any_space, any_space),
+        scratch_shapes=[pltpu.VMEM((tok, D), bf16), dma((2, SPLIT)), dma((1,))],
         compiler_params=pltpu.CompilerParams(vmem_limit_bytes=16 * 1024 * 1024),
     )(up_held, down_held, parts)
 

time: 180 us -> 177 us (0.983)
  Pallas kernels: 179 us -> 177 us
where the time goes in v2:
time: 177 us
  Pallas kernels  177 us (100%)
    pallas_call x1, Pallas kernels, body(): pl.pallas_call(functools.partial(kernel, G, F, T), name='handoff', out_sh...  171 us
    pallas_call x1, Pallas kernels, body(): pl.pallas_call(functools.partial(finish, G, F), name='finish', out_shape=...  6.06 us

profile of v2, /device:TPU:0, one launch (start us, length us, event | category | flops | bytes accessed | tf_op | source)
XLA Modules:
  0.0 177.3 jit_solution(18018489135665211874)
XLA Ops:
  0.6 170.6 %handoff.1 = (bf16[2048,2048]{1,0:T(8,128)(2,1)S(1)}, bf16[2048,2048]{1,0:T(8,128)(2,1)S(1)}, bf16[4,8,144,256]{3,2,1,0:T(8,128)(2,1)S(1)}) custom-call(bf16[144,2048]{1,0:T(8,128)(2,1)} %tok_in.1, f32[1,128]{1,0:T(1,128)} %bitcast.1, f32[128,4096]{1,0:T(8,128)} %up_in.1, f32[128,4096]{1,0:T(8,128)} %down_in.1), custom_call_target="tpu_custom_call" | custom-call | tf_op jit(solution)/shard_map/handoff/pallas_call | solution.py:439
  171.3 6.1 %finish.1 = (bf16[2048,2048]{1,0:T(8,128)(2,1)}, bf16[2048,2048]{1,0:T(8,128)(2,1)}, bf16[144,2048]{1,0:T(8,128)(2,1)}) custom-call(bf16[2048,2048]{1,0:T(8,128)(2,1)S(1)} %get-tuple-element.6.up_held, bf16[2048,2048]{1,0:T(8,128)(2,1)S(1)} %get-tuple-element.7.down_held, bf16[4,8,144,256]{3,2,1,0:T(8,128)(2,1)S(1)} %get-tuple-element.8.parts), custom_call_target="tpu_custom_call" | custom-call | tf_op jit(solution)/shard_map/finish/pallas_call | solution.py:463

commit v3 on v2

--- a/solution.py
+++ b/solution.py
@@ -178,43 +178,57 @@
         if columns:
             send(m, origin, q, sendy, "cross", mate, columns)
 
-    def own_chunk(m, q, columns):
+    def own_chunk(m, q, columns, pair=True):
         left(m, f, q)
         right(m, f, q)
-        if not columns:
-            send(m, f, q, sendy, "pair", mate)
-        elif columns[0] > 0:
-            send(m, f, q, sendy, "pair", mate, (0, columns[0]))
+        if pair and columns[:1] != (0,):
+            send(m, f, q, sendy, "pair", mate, (0, columns[0]) if columns else whole)
         across(m, f, q, columns)
 
     def own(m):
         def near(columns):
             def step(q):
-                if m == 0:
+                @pl.when(jnp.logical_not(home))
+                def _():
+                    arrived(m, f, q)
+                    if m == 0:
+                        own_chunk(m, q, columns)
+                if m > 0:
+                    own_chunk(m, q, columns, False)
+            return step
+
+        def far(q):
+            arrived(m, f, q)
+            own_chunk(m, q, whole)
+
+        shared, rest = over_line(m)
+        if m == 0:
+            for low, high, columns in shared:
+                loop(low, high, near(columns))
+            loop(rest[0], rest[1], near(whole))
+            loop(C, NQ, far)
+        else:
+            for low, high, columns in over_pair(m):
+                def step(q):
                     @pl.when(jnp.logical_not(home))
                     def _():
                         arrived(m, f, q)
-                        own_chunk(m, q, columns)
-                else:
-                    @pl.when(jnp.logical_not(home))
-                    def _():
-                        arrived(m, f, q)
-                    own_chunk(m, q, columns)
-            return step
-
-        def far(q):
-            arrived(m, f, q)
-            own_chunk(m, q, whole)
-
-        shared, rest = over_line(m)
-        for low, high, columns in shared:
-            loop(low, high, near(columns))
-        if m == 0:
+                    send(m, f, q, sendy, "pair", mate, columns)
+                loop(low, high, step)
+
+            loop(C, NQ, far)
+
+            def step(columns):
+                def go(q):
+                    own_chunk(m, q, columns, False)
+                return go
+            for low, high, columns in shared:
+                if columns:
+                    loop(low, high, step(columns))
             loop(rest[0], rest[1], near(whole))
-            loop(C, NQ, far)
-        else:
-            loop(C, NQ, far)
-            loop(rest[0], rest[1], near(whole))
+            for low, high, columns in shared:
+                if not columns:
+                    loop(low, high, step(columns))
 
     def mated(m):
         for low, high, columns in over_pair(m):
@@ -249,16 +263,22 @@
             return step
 
         shared, rest = over_line(m)
-        for low, high, columns in shared:
-            loop(low, high, both("line", columns))
         if m == 0:
+            for low, high, columns in shared:
+                loop(low, high, both("line", columns))
             loop(rest[0], rest[1], both("line", whole))
             loop(C, NQ, both("line", whole))
         else:
             loop(C, NQ, both("line", whole))
             if between is not None:
                 between()
+            for low, high, columns in shared:
+                if columns:
+                    loop(low, high, both("line", columns))
             loop(rest[0], rest[1], both("line", whole))
+            for low, high, columns in shared:
+                if not columns:
+                    loop(low, high, both("line", columns))
         if eager is not None:
             eager()
         for low, high, columns in over_pair(m):

time: 177 us -> 176 us (level)
  Pallas kernels: 177 us -> 175 us
where the time goes in v3:
time: 176 us
  Pallas kernels  175 us (99%)
    pallas_call x1, Pallas kernels, body(): pl.pallas_call(functools.partial(kernel, G, F, T), name='handoff', out_sh...  169 us
    pallas_call x1, Pallas kernels, body(): pl.pallas_call(functools.partial(finish, G, F), name='finish', out_shape=...  6.06 us

profile of v3, /device:TPU:0, one launch (start us, length us, event | category | flops | bytes accessed | tf_op | source)
XLA Modules:
  0.0 176.1 jit_solution(3109351390685111542)
XLA Ops:
  0.6 169.4 %handoff.1 = (bf16[2048,2048]{1,0:T(8,128)(2,1)S(1)}, bf16[2048,2048]{1,0:T(8,128)(2,1)S(1)}, bf16[4,8,144,256]{3,2,1,0:T(8,128)(2,1)S(1)}) custom-call(bf16[144,2048]{1,0:T(8,128)(2,1)} %tok_in.1, f32[1,128]{1,0:T(1,128)} %bitcast.1, f32[128,4096]{1,0:T(8,128)} %up_in.1, f32[128,4096]{1,0:T(8,128)} %down_in.1), custom_call_target="tpu_custom_call" | custom-call | tf_op jit(solution)/shard_map/handoff/pallas_call | solution.py:459
  170.0 6.1 %finish.1 = (bf16[2048,2048]{1,0:T(8,128)(2,1)}, bf16[2048,2048]{1,0:T(8,128)(2,1)}, bf16[144,2048]{1,0:T(8,128)(2,1)}) custom-call(bf16[2048,2048]{1,0:T(8,128)(2,1)S(1)} %get-tuple-element.6.up_held, bf16[2048,2048]{1,0:T(8,128)(2,1)S(1)} %get-tuple-element.7.down_held, bf16[4,8,144,256]{3,2,1,0:T(8,128)(2,1)S(1)} %get-tuple-element.8.parts), custom_call_target="tpu_custom_call" | custom-call | tf_op jit(solution)/shard_map/finish/pallas_call | solution.py:483

commit v4 on v3

--- a/solution.py
+++ b/solution.py
@@ -23,7 +23,7 @@
 def kernel(G, F, T, tok_in, gain_in, up_in, down_in, up_full, down_full, part,
            wide, narrow, raw, nrm, hid, stage,
            recv, dup, cross, cross_down, sendl, sendr, sendy, send0, tok_recv, tok_send,
-           part_recv, part_send, local_sem, load_sem):
+           part_recv, part_send, local_sem, load_sem, ready):
     gr, f, tp = lax.axis_index("gr"), lax.axis_index("fs"), lax.axis_index("tp")
     full = (up_full, down_full)
     A = F // 2
@@ -47,26 +47,43 @@
         rows = pl.ds(c * CH, CH)
         return pltpu.make_async_copy(weights[m].at[rows], wide.at[m, rows], load_sem.at[m, c])
 
-    for c in range(C):
+    load(0, 0).start()
+    barrier = pltpu.get_barrier_semaphore()
+
+    @pl.when(a < A - 1)
+    def _():
+        pl.semaphore_signal(barrier, inc=1, device_id=(gr, f + 2, tp), device_id_type=MESH)
+
+    @pl.when(y == 0)
+    def _():
+        pl.semaphore_signal(barrier, inc=1, device_id=(gr, mate, tp), device_id_type=MESH)
+
+    for kk in range(1, K):
+        @pl.when(kk > k)
+        def _():
+            pl.semaphore_signal(barrier, inc=1, device_id=at_k(kk), device_id_type=MESH)
+
+    token_load = pltpu.make_async_copy(tok_in, raw, local_sem.at[0])
+    for c in range(1, C):
         load(0, c).start()
-
-    barrier = pltpu.get_barrier_semaphore()
+    partners = (a > 0).astype(jnp.int32) + y + k
+
+    @pl.when(partners > 0)
+    def _():
+        pl.semaphore_wait(barrier, partners)
 
     @pl.when(a > 0)
     def _():
-        pl.semaphore_signal(barrier, inc=1, device_id=(gr, f - 2, tp), device_id_type=MESH)
-
-    @pl.when(a < A - 1)
-    def _():
-        pl.semaphore_signal(barrier, inc=1, device_id=(gr, f + 2, tp), device_id_type=MESH)
-    pl.semaphore_signal(barrier, inc=1, device_id=(gr, mate, tp), device_id_type=MESH)
-    for d in range(1, K):
-        pl.semaphore_signal(barrier, inc=1, device_id=at_k((k + d) % K), device_id_type=MESH)
-
-    token_load = pltpu.make_async_copy(tok_in, raw, local_sem.at[0])
-    for c in range(C):
-        load(1, c).start()
-    token_load.start()
+        pl.semaphore_signal(ready.at[0], inc=1, device_id=(gr, f - 2, tp), device_id_type=MESH)
+
+    @pl.when(y == 1)
+    def _():
+        pl.semaphore_signal(ready.at[1], inc=1, device_id=(gr, mate, tp), device_id_type=MESH)
+
+    for kk in range(K - 1):
+        @pl.when(kk < k)
+        def _():
+            pl.semaphore_signal(ready.at[2], inc=1, device_id=at_k(kk), device_id_type=MESH)
 
     def rows_of(origin, g, c):
         return pl.ds(pl.multiple_of(g * (F * R) + origin * R + c * CH, CH), CH)
@@ -178,8 +195,9 @@
         if columns:
             send(m, origin, q, sendy, "cross", mate, columns)
 
-    def own_chunk(m, q, columns, pair=True):
-        left(m, f, q)
+    def own_chunk(m, q, columns, pair=True, down_line=True):
+        if down_line:
+            left(m, f, q)
         right(m, f, q)
         if pair and columns[:1] != (0,):
             send(m, f, q, sendy, "pair", mate, (0, columns[0]) if columns else whole)
@@ -238,7 +256,7 @@
                 right(m, mate, q, "pair", columns)
             loop(low, high, step)
 
-    def line(m, s, between=None, eager=None):
+    def line(m, s, between=None, eager=None, closing=None):
         below, above = a - 1 - s, a + 1 + s
 
         def both(side, columns):
@@ -276,11 +294,13 @@
                 if columns:
                     loop(low, high, both("line", columns))
             loop(rest[0], rest[1], both("line", whole))
+            if eager is not None:
+                eager()
             for low, high, columns in shared:
                 if not columns:
                     loop(low, high, both("line", columns))
-        if eager is not None:
-            eager()
+        if closing is not None:
+            closing()
         for low, high, columns in over_pair(m):
             loop(low, high, both("pair", columns))
 
@@ -299,15 +319,35 @@
 
     for c in range(C):
         cast(0, c)
-        if c == 0:
-            pl.semaphore_wait(barrier, K + (a > 0).astype(jnp.int32) + (a < A - 1).astype(jnp.int32))
 
         @pl.when(home)
         def _():
-            pf, shared = share[0]
-            own_chunk(0, c, () if c < pf else (shared if c == pf else 0, W))
+            left(0, f, c)
+
+    for c in range(C):
+        load(1, c).start()
+    token_load.start()
+
+    @pl.when(k < K - 1)
+    def _():
+        pl.semaphore_wait(ready.at[2], K - 1 - k)
+    for c in range(C):
         for b in range(G):
             hand(0, b, c)
+
+    @pl.when(y == 0)
+    def _():
+        pl.semaphore_wait(ready.at[1], 1)
+
+    @pl.when(a < A - 1)
+    def _():
+        pl.semaphore_wait(ready.at[0], 1)
+
+    @pl.when(home)
+    def _():
+        pf, shared = share[0]
+        for c in range(C):
+            own_chunk(0, c, () if c < pf else (shared if c == pf else 0, W), True, False)
 
     own(0)
     token_load.wait()
@@ -373,7 +413,6 @@
             step(a + 1 + (A - 2))
 
     def early():
-        lower_ring(A - 2, 0, G - 1)
         if halves == 2:
             ends(lambda origin_a: lower_half(origin_a, y))
 
@@ -397,7 +436,7 @@
 
     loop(0, G, lambda i: lower(a, G - 1 - i))
     loop(1, A - 2, lambda s: line(1, s, between=lambda: lower_ring(s - 1)))
-    line(1, A - 2, between=lambda: lower_ring(A - 3), eager=early)
+    line(1, A - 2, between=lambda: lower_ring(A - 3), eager=lambda: lower_ring(A - 2, 0, G - 1), closing=early)
     late()
 
     await_rows(part, K - 1, part_recv.at[0])
@@ -475,7 +514,7 @@
             pltpu.VMEM((A * G, K * tok, 2 * R), bf16),
             dma((2, A, NQ)), dma((2, A, pairs)), dma((1,)), dma((A, G)),
             dma((1,)), dma((1,)), dma((1,)), dma((1,)), dma((1,)), dma((1,)),
-            dma((1,)), dma((1,)), dma((1,)), dma((2, C)),
+            dma((1,)), dma((1,)), dma((1,)), dma((2, C)), pltpu.SemaphoreType.REGULAR((3,)),
         ],
         compiler_params=pltpu.CompilerParams(
             collective_id=0, has_side_effects=True, vmem_limit_bytes=41 * 1024 * 1024),

time: 176 us -> 176 us (level)
  no operation moved by 1% of the time
where the time goes in v4:
time: 176 us; the launch traced here: 175 us
  Pallas kernels  175 us (99%)
    pallas_call x1, Pallas kernels, body(): pl.pallas_call(functools.partial(kernel, G, F, T), name='handoff', out_sh...  169 us
    pallas_call x1, Pallas kernels, body(): pl.pallas_call(functools.partial(finish, G, F), name='finish', out_shape=...  6.06 us

profile of v4, /device:TPU:0, one launch (start us, length us, event | category | flops | bytes accessed | tf_op | source)
XLA Modules:
  0.0 175.4 jit_solution(3048029209779990949)
XLA Ops:
  0.6 168.7 %handoff.1 = (bf16[2048,2048]{1,0:T(8,128)(2,1)S(1)}, bf16[2048,2048]{1,0:T(8,128)(2,1)S(1)}, bf16[4,8,144,256]{3,2,1,0:T(8,128)(2,1)S(1)}) custom-call(bf16[144,2048]{1,0:T(8,128)(2,1)} %tok_in.1, f32[1,128]{1,0:T(1,128)} %bitcast.1, f32[128,4096]{1,0:T(8,128)} %up_in.1, f32[128,4096]{1,0:T(8,128)} %down_in.1), custom_call_target="tpu_custom_call" | custom-call | tf_op jit(solution)/shard_map/handoff/pallas_call | solution.py:498
  169.3 6.1 %finish.1 = (bf16[2048,2048]{1,0:T(8,128)(2,1)}, bf16[2048,2048]{1,0:T(8,128)(2,1)}, bf16[144,2048]{1,0:T(8,128)(2,1)}) custom-call(bf16[2048,2048]{1,0:T(8,128)(2,1)S(1)} %get-tuple-element.6.up_held, bf16[2048,2048]{1,0:T(8,128)(2,1)S(1)} %get-tuple-element.7.down_held, bf16[4,8,144,256]{3,2,1,0:T(8,128)(2,1)S(1)} %get-tuple-element.8.parts), custom_call_target="tpu_custom_call" | custom-call | tf_op jit(solution)/shard_map/finish/pallas_call | solution.py:522

commit v5 on v4

--- a/solution.py
+++ b/solution.py
@@ -44,8 +44,8 @@
         return (kk // T, f, kk % T)
 
     def load(m, c):
-        rows = pl.ds(c * CH, CH)
-        return pltpu.make_async_copy(weights[m].at[rows], wide.at[m, rows], load_sem.at[m, c])
+        rows = pl.ds(c * CH, CH) if m == 0 else pl.ds(0, R)
+        return pltpu.make_async_copy(weights[m].at[rows], wide.at[m, rows], load_sem.at[c if m == 0 else C])
 
     load(0, 0).start()
     barrier = pltpu.get_barrier_semaphore()
@@ -83,7 +83,7 @@
     for kk in range(K - 1):
         @pl.when(kk < k)
         def _():
-            pl.semaphore_signal(ready.at[2], inc=1, device_id=at_k(kk), device_id_type=MESH)
+            pl.semaphore_signal(ready.at[1 + k], inc=1, device_id=at_k(kk), device_id_type=MESH)
 
     def rows_of(origin, g, c):
         return pl.ds(pl.multiple_of(g * (F * R) + origin * R + c * CH, CH), CH)
@@ -92,7 +92,8 @@
 
     def cast(m, c):
         rows = pl.ds(c * CH, CH)
-        load(m, c).wait()
+        if m == 0 or c == 0:
+            load(m, c).wait()
         value = wide[m, rows, :]
         if m == 0:
             value = value * column[c * CH:(c + 1) * CH]
@@ -145,7 +146,7 @@
         if side == "line":
             return recv.at[m, origin_a, q]
         if side == "pair":
-            return dup.at[m, origin_a, q]
+            return dup.at[m, origin_a]
         return cross.at[0] if m == 0 else cross_down.at[origin_a, q // C]
 
     whole = (0, W)
@@ -195,13 +196,15 @@
         if columns:
             send(m, origin, q, sendy, "cross", mate, columns)
 
-    def own_chunk(m, q, columns, pair=True, down_line=True):
-        if down_line:
-            left(m, f, q)
-        right(m, f, q)
+    def own_across(m, q, columns, pair=True):
         if pair and columns[:1] != (0,):
             send(m, f, q, sendy, "pair", mate, (0, columns[0]) if columns else whole)
         across(m, f, q, columns)
+
+    def own_chunk(m, q, columns, pair=True):
+        left(m, f, q)
+        right(m, f, q)
+        own_across(m, q, columns, pair)
 
     def own(m):
         def near(columns):
@@ -249,9 +252,9 @@
                     loop(low, high, step(columns))
 
     def mated(m):
+        await_rows(full[m], pair_rows(m), dup.at[m, a])
         for low, high, columns in over_pair(m):
             def step(q):
-                arrived(m, mate, q, "pair", columns)
                 left(m, mate, q, "pair", columns)
                 right(m, mate, q, "pair", columns)
             loop(low, high, step)
@@ -263,7 +266,8 @@
             sent = columns if side == "pair" else whole
 
             def pass_on(origin, q, onward):
-                arrived(m, origin, q, side, sent)
+                if side == "line":
+                    arrived(m, origin, q)
                 onward(m, origin, q, side, sent)
                 if side == "line":
                     across(m, origin, q, columns)
@@ -301,6 +305,10 @@
                     loop(low, high, both("line", columns))
         if closing is not None:
             closing()
+        for origin_a in (below, above):
+            @pl.when(jnp.logical_and(origin_a >= 0, origin_a < A))
+            def _():
+                await_rows(full[m], pair_rows(m), dup.at[m, origin_a])
         for low, high, columns in over_pair(m):
             loop(low, high, both("pair", columns))
 
@@ -317,6 +325,10 @@
         def _():
             await_rows(down_full, C * CH, cross_down.at[origin_a, gi])
 
+    def sharing(c):
+        pf, shared = share[0]
+        return () if c < pf else (shared if c == pf else 0, W)
+
     for c in range(C):
         cast(0, c)
 
@@ -324,13 +336,20 @@
         def _():
             left(0, f, c)
 
-    for c in range(C):
-        load(1, c).start()
+            @pl.when(y == 1)
+            def _():
+                own_across(0, c, sharing(c))
+
+    load(1, 0).start()
     token_load.start()
 
-    @pl.when(k < K - 1)
-    def _():
-        pl.semaphore_wait(ready.at[2], K - 1 - k)
+    def meet(kk):
+        @pl.when(kk > k)
+        def _():
+            pl.semaphore_wait(ready.at[1 + kk], 1)
+
+    for b in range(G):
+        meet(tp * G + b)
     for c in range(C):
         for b in range(G):
             hand(0, b, c)
@@ -339,15 +358,19 @@
     def _():
         pl.semaphore_wait(ready.at[1], 1)
 
+        @pl.when(home)
+        def _():
+            for c in range(C):
+                own_across(0, c, sharing(c))
+
     @pl.when(a < A - 1)
     def _():
         pl.semaphore_wait(ready.at[0], 1)
 
-    @pl.when(home)
-    def _():
-        pf, shared = share[0]
-        for c in range(C):
-            own_chunk(0, c, () if c < pf else (shared if c == pf else 0, W), True, False)
+        @pl.when(home)
+        def _():
+            for c in range(C):
+                right(0, f, c)
 
     own(0)
     token_load.wait()
@@ -356,6 +379,10 @@
         cast(1, c)
         for b in range(G):
             hand(1, b, c)
+    for kk in range(1, K):
+        @pl.when(kk // G != tp)
+        def _():
+            meet(kk)
     tokens()
     mated(0)
     loop(0, A - 2, lambda s: line(0, s))
@@ -393,6 +420,8 @@
         for d in range(1, K):
             part_copy(d, block, columns).start()
 
+    far = jnp.where(2 * a < A, A - 1, 0)
+
     def lower(origin_a, gi):
         settle_down(origin_a, gi)
         g = (gr + gi) % G
@@ -403,40 +432,43 @@
         rows = pl.ds(pl.multiple_of(gr * (F * R) + (origin_a * 2 + side) * R, R), R)
         multiply(origin_a * G + gr, rows, pl.ds(pl.multiple_of(side * R, R), R))
 
-    def ends(step):
-        @pl.when(a - 1 - (A - 2) >= 0)
-        def _():
-            step(a - 1 - (A - 2))
-
-        @pl.when(a + 1 + (A - 2) < A)
-        def _():
-            step(a + 1 + (A - 2))
+    def at_far(step):
+        for end in (0, A - 1):
+            @pl.when(far == end)
+            def _():
+                step(end)
 
     def early():
         if halves == 2:
-            ends(lambda origin_a: lower_half(origin_a, y))
+            at_far(lambda origin_a: lower_half(origin_a, y))
 
     def late():
         if halves == 2:
-            def step(origin_a):
-                settle_down(origin_a, 0)
-                lower_half(origin_a, 1 - y)
-            ends(step)
+            settle_down(far, 0)
+            at_far(lambda origin_a: lower_half(origin_a, 1 - y))
         else:
-            lower_ring(A - 2, G - 1, G)
-
-    def lower_ring(s, low=0, high=G):
+            lower(far, 0)
+
+    def lower_ring(s, last=True):
+        def blocks(origin_a):
+            loop(0, G - 1, lambda i: lower(origin_a, G - 1 - i))
+
+            if last:
+                @pl.when(origin_a != far)
+                def _():
+                    lower(origin_a, 0)
+
         @pl.when(a - 1 - s >= 0)
         def _():
-            loop(low, high, lambda i: lower(a - 1 - s, G - 1 - i))
+            blocks(a - 1 - s)
 
         @pl.when(a + 1 + s < A)
         def _():
-            loop(low, high, lambda i: lower(a + 1 + s, G - 1 - i))
+            blocks(a + 1 + s)
 
     loop(0, G, lambda i: lower(a, G - 1 - i))
     loop(1, A - 2, lambda s: line(1, s, between=lambda: lower_ring(s - 1)))
-    line(1, A - 2, between=lambda: lower_ring(A - 3), eager=lambda: lower_ring(A - 2, 0, G - 1), closing=early)
+    line(1, A - 2, between=lambda: lower_ring(A - 3), eager=lambda: lower_ring(A - 2, False), closing=early)
     late()
 
     await_rows(part, K - 1, part_recv.at[0])
@@ -490,7 +522,6 @@
     A, K = F // 2, G * T
     C = R // min(CHUNK, R)
     NQ = G * C
-    pairs = max(1, max(pf + (shared > 0) for pf, shared in pair_share(NQ, W)))
     bf16 = jnp.bfloat16
     any_space = pl.BlockSpec(memory_space=pl.ANY)
     vmem_space = pl.BlockSpec(memory_space=pltpu.VMEM)
@@ -512,9 +543,9 @@
             pltpu.VMEM((K * tok, D), bf16),
             pltpu.VMEM((K * tok, W), bf16),
             pltpu.VMEM((A * G, K * tok, 2 * R), bf16),
-            dma((2, A, NQ)), dma((2, A, pairs)), dma((1,)), dma((A, G)),
+            dma((2, A, NQ)), dma((2, A)), dma((1,)), dma((A, G)),
             dma((1,)), dma((1,)), dma((1,)), dma((1,)), dma((1,)), dma((1,)),
-            dma((1,)), dma((1,)), dma((1,)), dma((2, C)), pltpu.SemaphoreType.REGULAR((3,)),
+            dma((1,)), dma((1,)), dma((1,)), dma((C + 1,)), pltpu.SemaphoreType.REGULAR((K + 1,)),
         ],
         compiler_params=pltpu.CompilerParams(
             collective_id=0, has_side_effects=True, vmem_limit_bytes=41 * 1024 * 1024),

time: 176 us -> 175 us (level)
  no operation moved by 1% of the time
where the time goes in v5:
time: 175 us
  Pallas kernels  175 us (100%)
    pallas_call x1, Pallas kernels, body(): pl.pallas_call(functools.partial(kernel, G, F, T), name='handoff', out_sh...  169 us
    pallas_call x1, Pallas kernels, body(): pl.pallas_call(functools.partial(finish, G, F), name='finish', out_shape=...  6.06 us

profile of v5, /device:TPU:0, one launch (start us, length us, event | category | flops | bytes accessed | tf_op | source)
XLA Modules:
  0.0 175.3 jit_solution(6966026468654739795)
XLA Ops:
  0.6 168.6 %handoff.1 = (bf16[2048,2048]{1,0:T(8,128)(2,1)S(1)}, bf16[2048,2048]{1,0:T(8,128)(2,1)S(1)}, bf16[4,8,144,256]{3,2,1,0:T(8,128)(2,1)S(1)}) custom-call(bf16[144,2048]{1,0:T(8,128)(2,1)} %tok_in.1, f32[1,128]{1,0:T(1,128)} %bitcast.1, f32[128,4096]{1,0:T(8,128)} %up_in.1, f32[128,4096]{1,0:T(8,128)} %down_in.1), custom_call_target="tpu_custom_call" | custom-call | tf_op jit(solution)/shard_map/handoff/pallas_call | solution.py:529
  169.3 6.1 %finish.1 = (bf16[2048,2048]{1,0:T(8,128)(2,1)}, bf16[2048,2048]{1,0:T(8,128)(2,1)}, bf16[144,2048]{1,0:T(8,128)(2,1)}) custom-call(bf16[2048,2048]{1,0:T(8,128)(2,1)S(1)} %get-tuple-element.6.up_held, bf16[2048,2048]{1,0:T(8,128)(2,1)S(1)} %get-tuple-element.7.down_held, bf16[4,8,144,256]{3,2,1,0:T(8,128)(2,1)S(1)} %get-tuple-element.8.parts), custom_call_target="tpu_custom_call" | custom-call | tf_op jit(solution)/shard_map/finish/pallas_call | solution.py:553

commit v6 on v5

--- a/solution.py
+++ b/solution.py
@@ -15,8 +15,8 @@
 
 def pair_share(count, width):
     share = []
-    for quarters in (count * 5 // 8, count * 6 // 8):
-        share.append((quarters // 4, quarters % 4 * (width // 4)))
+    for eighths in (count * 10 // 8, count * 11 // 8):
+        share.append((eighths // 8, eighths % 8 * (width // 8)))
     return share
 
 
@@ -160,6 +160,8 @@
     def await_rows(ref, count, sem):
         if count > 0:
             rows = ref.at[pl.ds(0, count)]
+            if len(ref.shape) == 2 and count % 8:
+                rows = ref.at[pl.ds(0, 2 * count), pl.ds(0, ref.shape[1] // 2)]
             pltpu.make_async_copy(rows, rows, sem).wait()
 
     def arrived(m, origin, q, side="line", columns=whole):
@@ -416,9 +418,9 @@
         value = lax.dot_general(hid[...], down_full[rows, :], (((1,), (1,)), ((), ())),
                                 preferred_element_type=jnp.float32)
         stage[block, :, columns] = value.astype(jnp.bfloat16)
-        part[K - 1, block, :, columns] = stage[block, mine, columns]
         for d in range(1, K):
             part_copy(d, block, columns).start()
+        part[K - 1, block, :, columns] = stage[block, mine, columns]
 
     far = jnp.where(2 * a < A, A - 1, 0)
 
@@ -471,8 +473,6 @@
     line(1, A - 2, between=lambda: lower_ring(A - 3), eager=lambda: lower_ring(A - 2, False), closing=early)
     late()
 
-    await_rows(part, K - 1, part_recv.at[0])
-    await_rows(part, K - 1, part_send.at[0])
     await_rows(nrm, (K - 1) * tok, tok_send.at[0])
     pairs = pair_rows(0) + pair_rows(1)
     await_rows(up_full, 2 * NQ * CH, sendy.at[0])
@@ -487,6 +487,8 @@
     lax.fori_loop(0, jnp.where(a > 0, A - a, 0), drain(sendl, 2 * NQ * CH + pairs), 0)
     lax.fori_loop(0, jnp.where(a < A - 1, a + 1, 0), drain(sendr, 2 * NQ * CH + pairs), 0)
     lax.fori_loop(0, jnp.where(home, G - 1, G), drain(send0, 2 * R), 0)
+    await_rows(part, K - 1, part_recv.at[0])
+    await_rows(part, K - 1, part_send.at[0])
 
 
 def finish(G, F, up_held, down_held, parts, up_out, down_out, out_ref, summed, sems, out_sem):

time: 175 us -> 175 us (level)
  no operation moved by 1% of the time
where the time goes in v6:
time: 175 us
  Pallas kernels  174 us (99%)
    pallas_call x1, Pallas kernels, body(): pl.pallas_call(functools.partial(kernel, G, F, T), name='handoff', out_sh...  168 us
    pallas_call x1, Pallas kernels, body(): pl.pallas_call(functools.partial(finish, G, F), name='finish', out_shape=...  6.06 us

profile of v6, /device:TPU:0, one launch (start us, length us, event | category | flops | bytes accessed | tf_op | source)
XLA Modules:
  0.0 174.9 jit_solution(6001457864339459628)
XLA Ops:
  0.6 168.2 %handoff.1 = (bf16[2048,2048]{1,0:T(8,128)(2,1)S(1)}, bf16[2048,2048]{1,0:T(8,128)(2,1)S(1)}, bf16[4,8,144,256]{3,2,1,0:T(8,128)(2,1)S(1)}) custom-call(bf16[144,2048]{1,0:T(8,128)(2,1)} %tok_in.1, f32[1,128]{1,0:T(1,128)} %bitcast.1, f32[128,4096]{1,0:T(8,128)} %up_in.1, f32[128,4096]{1,0:T(8,128)} %down_in.1), custom_call_target="tpu_custom_call" | custom-call | tf_op jit(solution)/shard_map/handoff/pallas_call | solution.py:531
  168.8 6.1 %finish.1 = (bf16[2048,2048]{1,0:T(8,128)(2,1)}, bf16[2048,2048]{1,0:T(8,128)(2,1)}, bf16[144,2048]{1,0:T(8,128)(2,1)}) custom-call(bf16[2048,2048]{1,0:T(8,128)(2,1)S(1)} %get-tuple-element.6.up_held, bf16[2048,2048]{1,0:T(8,128)(2,1)S(1)} %get-tuple-element.7.down_held, bf16[4,8,144,256]{3,2,1,0:T(8,128)(2,1)S(1)} %get-tuple-element.8.parts), custom_call_target="tpu_custom_call" | custom-call | tf_op jit(solution)/shard_map/finish/pallas_call | solution.py:555

commit v7 on v6

--- a/solution.py
+++ b/solution.py
@@ -104,6 +104,11 @@
             def _():
                 full[m][rows_of(f, gr, c), :] = value[:, b * W:(b + 1) * W]
 
+    batch = 2 if C % 2 == 0 else 1
+
+    def slot(q):
+        return jnp.where(q < C, q, C + (q - C) // batch)
+
     def hand(m, b, c):
         kk = tp * G + b
         q = ((gr - kk // T + G) % G) * C + c
@@ -113,7 +118,7 @@
             copy = pltpu.make_async_remote_copy(
                 src_ref=narrow.at[m, pl.ds(c * CH, CH), pl.ds(b * W, W)],
                 dst_ref=full[m].at[rows_of(f, gr, c)],
-                send_sem=send0.at[0], recv_sem=recv.at[m, a, q],
+                send_sem=send0.at[0], recv_sem=recv.at[m, a, slot(q)],
                 device_id=at_k(kk), device_id_type=MESH)
             copy.start()
 
@@ -144,7 +149,7 @@
 
     def landing(m, origin_a, side, q):
         if side == "line":
-            return recv.at[m, origin_a, q]
+            return recv.at[m, origin_a, slot(q)]
         if side == "pair":
             return dup.at[m, origin_a]
         return cross.at[0] if m == 0 else cross_down.at[origin_a, q // C]
@@ -164,9 +169,17 @@
                 rows = ref.at[pl.ds(0, 2 * count), pl.ds(0, ref.shape[1] // 2)]
             pltpu.make_async_copy(rows, rows, sem).wait()
 
-    def arrived(m, origin, q, side="line", columns=whole):
-        ref = chunk(m, origin, q, columns)
-        pltpu.make_async_copy(ref, ref, landing(m, origin // 2, side, q)).wait()
+    def arrived(m, origin, q):
+        sem = landing(m, origin // 2, "line", q)
+
+        @pl.when(q < C)
+        def _():
+            ref = chunk(m, origin, q, whole)
+            pltpu.make_async_copy(ref, ref, sem).wait()
+
+        @pl.when(jnp.logical_and(q >= C, (q - C) % batch == 0))
+        def _():
+            await_rows(full[m], batch * CH, sem)
 
     def left(m, origin, q, side="line", columns=whole):
         @pl.when(a > 0)
@@ -545,7 +558,7 @@
             pltpu.VMEM((K * tok, D), bf16),
             pltpu.VMEM((K * tok, W), bf16),
             pltpu.VMEM((A * G, K * tok, 2 * R), bf16),
-            dma((2, A, NQ)), dma((2, A)), dma((1,)), dma((A, G)),
+            dma((2, A, C + (NQ - C) // (2 if C % 2 == 0 else 1))), dma((2, A)), dma((1,)), dma((A, G)),
             dma((1,)), dma((1,)), dma((1,)), dma((1,)), dma((1,)), dma((1,)),
             dma((1,)), dma((1,)), dma((1,)), dma((C + 1,)), pltpu.SemaphoreType.REGULAR((K + 1,)),
         ],

time: 175 us -> 175 us (level)
  no operation moved by 1% of the time
where the time goes in v7:
time: 175 us
  Pallas kernels  174 us (99%)
    pallas_call x1, Pallas kernels, body(): pl.pallas_call(functools.partial(kernel, G, F, T), name='handoff', out_sh...  168 us
    pallas_call x1, Pallas kernels, body(): pl.pallas_call(functools.partial(finish, G, F), name='finish', out_shape=...  6.06 us

profile of v7, /device:TPU:0, one launch (start us, length us, event | category | flops | bytes accessed | tf_op | source)
XLA Modules:
  0.0 174.8 jit_solution(10084188967811641412)
XLA Ops:
  0.6 168.1 %handoff.1 = (bf16[2048,2048]{1,0:T(8,128)(2,1)S(1)}, bf16[2048,2048]{1,0:T(8,128)(2,1)S(1)}, bf16[4,8,144,256]{3,2,1,0:T(8,128)(2,1)S(1)}) custom-call(bf16[144,2048]{1,0:T(8,128)(2,1)} %tok_in.1, f32[1,128]{1,0:T(1,128)} %bitcast.1, f32[128,4096]{1,0:T(8,128)} %up_in.1, f32[128,4096]{1,0:T(8,128)} %down_in.1), custom_call_target="tpu_custom_call" | custom-call | tf_op jit(solution)/shard_map/handoff/pallas_call | solution.py:544
  168.7 6.1 %finish.1 = (bf16[2048,2048]{1,0:T(8,128)(2,1)}, bf16[2048,2048]{1,0:T(8,128)(2,1)}, bf16[144,2048]{1,0:T(8,128)(2,1)}) custom-call(bf16[2048,2048]{1,0:T(8,128)(2,1)S(1)} %get-tuple-element.6.up_held, bf16[2048,2048]{1,0:T(8,128)(2,1)S(1)} %get-tuple-element.7.down_held, bf16[4,8,144,256]{3,2,1,0:T(8,128)(2,1)S(1)} %get-tuple-element.8.parts), custom_call_target="tpu_custom_call" | custom-call | tf_op jit(solution)/shard_map/finish/pallas_call | solution.py:568

commit v8 on v7

--- a/solution.py
+++ b/solution.py
@@ -64,26 +64,27 @@
             pl.semaphore_signal(barrier, inc=1, device_id=at_k(kk), device_id_type=MESH)
 
     token_load = pltpu.make_async_copy(tok_in, raw, local_sem.at[0])
+    partners = (a > 0).astype(jnp.int32) + y + k
+
+    @pl.when(partners > 0)
+    def _():
+        pl.semaphore_wait(barrier, partners)
+
+    @pl.when(a > 0)
+    def _():
+        pl.semaphore_signal(ready.at[0], inc=1, device_id=(gr, f - 2, tp), device_id_type=MESH)
+
+    @pl.when(y == 1)
+    def _():
+        pl.semaphore_signal(ready.at[1], inc=1, device_id=(gr, mate, tp), device_id_type=MESH)
+
+    for kk in range(K - 1):
+        @pl.when(kk < k)
+        def _():
+            pl.semaphore_signal(ready.at[1 + k], inc=1, device_id=at_k(kk), device_id_type=MESH)
+
     for c in range(1, C):
         load(0, c).start()
-    partners = (a > 0).astype(jnp.int32) + y + k
-
-    @pl.when(partners > 0)
-    def _():
-        pl.semaphore_wait(barrier, partners)
-
-    @pl.when(a > 0)
-    def _():
-        pl.semaphore_signal(ready.at[0], inc=1, device_id=(gr, f - 2, tp), device_id_type=MESH)
-
-    @pl.when(y == 1)
-    def _():
-        pl.semaphore_signal(ready.at[1], inc=1, device_id=(gr, mate, tp), device_id_type=MESH)
-
-    for kk in range(K - 1):
-        @pl.when(kk < k)
-        def _():
-            pl.semaphore_signal(ready.at[1 + k], inc=1, device_id=at_k(kk), device_id_type=MESH)
 
     def rows_of(origin, g, c):
         return pl.ds(pl.multiple_of(g * (F * R) + origin * R + c * CH, CH), CH)

time: 175 us -> 175 us (level)
  no operation moved by 1% of the time
where the time goes in v8:
time: 175 us
  Pallas kernels  174 us (99%)
    pallas_call x1, Pallas kernels, body(): pl.pallas_call(functools.partial(kernel, G, F, T), name='handoff', out_sh...  168 us
    pallas_call x1, Pallas kernels, body(): pl.pallas_call(functools.partial(finish, G, F), name='finish', out_shape=...  6.06 us

profile of v8, /device:TPU:0, one launch (start us, length us, event | category | flops | bytes accessed | tf_op | source)
XLA Modules:
  0.0 174.8 jit_solution(6876819521613901492)
XLA Ops:
  0.6 168.1 %handoff.1 = (bf16[2048,2048]{1,0:T(8,128)(2,1)S(1)}, bf16[2048,2048]{1,0:T(8,128)(2,1)S(1)}, bf16[4,8,144,256]{3,2,1,0:T(8,128)(2,1)S(1)}) custom-call(bf16[144,2048]{1,0:T(8,128)(2,1)} %tok_in.1, f32[1,128]{1,0:T(1,128)} %bitcast.1, f32[128,4096]{1,0:T(8,128)} %up_in.1, f32[128,4096]{1,0:T(8,128)} %down_in.1), custom_call_target="tpu_custom_call" | custom-call | tf_op jit(solution)/shard_map/handoff/pallas_call | solution.py:545
  168.7 6.1 %finish.1 = (bf16[2048,2048]{1,0:T(8,128)(2,1)}, bf16[2048,2048]{1,0:T(8,128)(2,1)}, bf16[144,2048]{1,0:T(8,128)(2,1)}) custom-call(bf16[2048,2048]{1,0:T(8,128)(2,1)S(1)} %get-tuple-element.6.up_held, bf16[2048,2048]{1,0:T(8,128)(2,1)S(1)} %get-tuple-element.7.down_held, bf16[4,8,144,256]{3,2,1,0:T(8,128)(2,1)S(1)} %get-tuple-element.8.parts), custom_call_target="tpu_custom_call" | custom-call | tf_op jit(solution)/shard_map/finish/pallas_call | solution.py:569
